TPU v7x, 256 devices: a whole 4x4x8 slice. The times are simulated.
256 devices in a mesh: ep: 64 (over z, y, core), tp: 4 (over x).
Axes of the slice: x: 4, y: 4, z: 8, core: 2. Of those that a mesh axis runs over, the one named last changes fastest.
Arguments:
- tokens_a: bfloat16 [8192, 2048], P('ep'), may hold values from -30 to 30
- attn_gain: float32 [2048], replicated, may hold values from 0.1 to 1.9
- w_query: bfloat16 [2048, 2048], P(None, 'tp'), may hold values from -2 to 2
- w_query_rot: bfloat16 [2048, 1024], P(None, 'tp'), may hold values from -0.125 to 0.125
- w_latent: bfloat16 [2048, 512], replicated, may hold values from -2 to 2
- w_key_rot: bfloat16 [2048, 32], replicated, may hold values from -0.125 to 0.125
- latent_gain: float32 [512], replicated, may hold values from 0.1 to 1.9
- w_key_up: bfloat16 [512, 2048], P(None, 'tp'), may hold values from -2 to 2
- w_value_up: bfloat16 [512, 2048], P(None, 'tp'), may hold values from -0.25 to 0.25
- w_output: bfloat16 [2048, 2048], P('tp'), may hold values from -0.125 to 0.125
- tokens_b: bfloat16 [16384, 2048], P('ep'), may hold values from -6 to 6
- ffn_gain: float32 [2048], replicated, may hold values from 0.1 to 1.9
- expert_ids: int32 [16384, 2], P('ep'), may hold values from 0 to 63, all different within a row; in each aligned block of 256 rows (0 to 255, 256 to 511, ...) at most 16 rows name the same one
- expert_weights: float32 [16384, 2], P('ep'), may hold values from 0.1 to 1
- w_gate: bfloat16 [64, 2048, 1024], P('ep', None, 'tp'), may hold values from -0.125 to 0.125
- w_up: bfloat16 [64, 2048, 1024], P('ep', None, 'tp'), may hold values from -0.125 to 0.125
- w_down: bfloat16 [64, 1024, 2048], P('ep', 'tp'), may hold values from -0.1875 to 0.1875
Outputs:
- mixed_a: bfloat16 [8192, 2048], P(('ep', 'tp'))
- mixed_b: bfloat16 [16384, 2048], P('ep', 'tp')
Inputs may be any that keep to these rules, and one draw needn't show every extreme that they name: `expert_ids`: each row names 2 different experts. In the 256 rows of one index of ep no expert is named more than 16 times, and in some such block one expert is named exactly 16 times.
All inputs are finite; a program needn't handle non-finite values.
Results may differ from a plain program's by a relative error of at most 0.012.
Values may be sent and summed in bfloat16 or wider, within the bound.
No kernel may reach another device: no remote copies, remote signals or barrier semaphores. Data moves between devices by JAX's collectives and lax.ppermute only.
A program may use at most 192 MiB of HBM per device.

v0:
```python
import jax
import jax.numpy as jnp
from jax import lax
from jax.sharding import PartitionSpec as P

NOPE = 64
ROPE = 32
VD = 64
epsilon = 1e-06
rope_base = 10000.0


def normalize(matrix, gain):
    floats = matrix.astype(jnp.float32)
    scaled = floats * lax.rsqrt(jnp.mean(floats * floats, axis=-1, keepdims=True) + epsilon)
    return scaled * gain


def rotate(vectors, positions):
    rot_width = vectors.shape[-1]
    half_width = rot_width // 2
    inverse = rope_base ** (-(jnp.arange(half_width, dtype=jnp.float32) * 2.0) / rot_width)
    angles = positions.astype(jnp.float32)[:, None] * inverse[None, :]
    cosine = jnp.cos(angles)[:, None, :]
    sine_part = jnp.sin(angles)[:, None, :]
    first_half = vectors[..., :half_width]
    second_half = vectors[..., half_width:]
    return jnp.concatenate(
        [
            first_half * cosine - second_half * sine_part,
            first_half * sine_part + second_half * cosine,
        ],
        axis=-1,
    )


def attention_half(
    tokens_a,
    attn_gain,
    w_query,
    w_query_rot,
    w_latent,
    w_key_rot,
    latent_gain,
    w_key_up,
    w_value_up,
    w_output,
):
    row_count = tokens_a.shape[0]
    head_count = w_query.shape[1] // NOPE
    offset = lax.axis_index("ep") * row_count
    positions = offset + jnp.arange(row_count, dtype=jnp.int32)
    normed = normalize(tokens_a, attn_gain).astype(jnp.bfloat16)
    query_plain = jnp.dot(normed, w_query, preferred_element_type=jnp.float32).astype(jnp.bfloat16)
    query_plain = query_plain.reshape(row_count, head_count, NOPE)
    turned = jnp.dot(normed, w_query_rot, preferred_element_type=jnp.float32).reshape(
        row_count, head_count, ROPE
    )
    query_rotated_rows = rotate(turned, positions).astype(jnp.bfloat16)
    latent = normalize(
        jnp.dot(normed, w_latent, preferred_element_type=jnp.float32), latent_gain
    ).astype(jnp.bfloat16)
    key_raw = jnp.dot(normed, w_key_rot, preferred_element_type=jnp.float32)[:, None, :]
    key_turned = rotate(key_raw, positions)[:, 0, :].astype(jnp.bfloat16)
    logit_scale = (NOPE + ROPE) ** (-0.5)
    key_plain = jnp.dot(latent, w_key_up, preferred_element_type=jnp.float32).astype(jnp.bfloat16)
    values = jnp.dot(latent, w_value_up, preferred_element_type=jnp.float32).astype(jnp.bfloat16)
    update_key_plain = lax.all_gather(key_plain, "ep", axis=0, tiled=True)
    update_values = lax.all_gather(values, "ep", axis=0, tiled=True)
    key_count = update_key_plain.shape[0]
    blocks = key_count // row_count
    key_blocks = update_key_plain.reshape(blocks, row_count, head_count, NOPE)
    value_blocks = update_values.reshape(blocks, row_count, head_count, VD)
    rotated_key_blocks = lax.all_gather(key_turned, "ep", axis=0, tiled=True).reshape(
        blocks, row_count, ROPE
    )
    score_matrix = (
        jnp.einsum("yvz,wrvz->yvwr", query_plain, key_blocks, preferred_element_type=jnp.float32)
        + jnp.einsum(
            "yjx,inx->yjin",
            query_rotated_rows,
            rotated_key_blocks,
            preferred_element_type=jnp.float32,
        )
    ) * logit_scale
    key_pos = jnp.arange(key_count, dtype=jnp.int32).reshape(blocks, row_count)
    allowed = key_pos[None, None, :, :] <= positions[:, None, None, None]
    masked = jnp.where(allowed, score_matrix, -1e30)
    block_max = jnp.max(masked, axis=-1)
    probs = jnp.where(allowed, jnp.exp(masked - block_max[..., None]), 0.0)
    block_total = jnp.sum(probs, axis=-1)
    block_out = jnp.einsum(
        "qhbk,bkhd->qhbd",
        probs.astype(jnp.bfloat16),
        value_blocks,
        preferred_element_type=jnp.float32,
    )
    run_max = jnp.full((row_count, head_count), -1e30, jnp.float32)
    new_max = jnp.maximum(run_max, jnp.max(block_max, axis=-1))
    new_factor = jnp.exp(block_max - new_max[..., None])
    new_total = jnp.sum(new_factor * block_total, axis=-1)
    new_out = jnp.sum(new_factor[..., None] * block_out, axis=2)
    attended = (
        (new_out / new_total[..., None]).astype(jnp.bfloat16).reshape(row_count, head_count * VD)
    )
    return lax.psum_scatter(
        jnp.dot(attended, w_output, preferred_element_type=jnp.float32).astype(jnp.bfloat16),
        "tp",
        scatter_dimension=0,
        tiled=True,
    )


def expert_half(tokens_b, ffn_gain, expert_ids, expert_weights, w_gate, w_up, w_down):
    row_count = tokens_b.shape[0]
    top_count = expert_ids.shape[1]
    expert_count = w_gate.shape[0] * lax.axis_size("ep")
    capacity = 2 * row_count * top_count // expert_count
    normed = normalize(tokens_b, ffn_gain).astype(jnp.bfloat16)
    flat_ids = expert_ids.reshape(-1)
    pair_count = flat_ids.shape[0]
    onehot = (flat_ids[:, None] == jnp.arange(expert_count, dtype=jnp.int32)[None, :]).astype(
        jnp.int32
    )
    before = jnp.cumsum(onehot, axis=0) - onehot
    slot_index = jnp.sum(before * onehot, axis=1)
    target = flat_ids * capacity + slot_index
    source_row = (
        jnp.zeros((expert_count * capacity,), jnp.int32)
        .at[target]
        .set(jnp.arange(pair_count, dtype=jnp.int32) // top_count)
    )
    occupied = jnp.zeros((expert_count * capacity,), jnp.int32).at[target].set(1)
    outgoing = jnp.where(occupied[:, None] > 0, normed[source_row], jnp.zeros((), jnp.bfloat16))
    outgoing = outgoing.reshape(expert_count, capacity, normed.shape[1])
    gate_weight = w_gate[0]
    up_weight = w_up[0]
    down_weight = w_down[0]
    arrived = lax.all_to_all(outgoing, "ep", split_axis=0, concat_axis=0, tiled=True)
    flat_rows = arrived.reshape(-1, arrived.shape[-1])
    gate_part = jnp.dot(flat_rows, gate_weight, preferred_element_type=jnp.float32)
    up_part = jnp.dot(flat_rows, up_weight, preferred_element_type=jnp.float32)
    hidden_rows = (jax.nn.silu(gate_part) * up_part).astype(jnp.bfloat16)
    hidden = hidden_rows.reshape(arrived.shape[0], arrived.shape[1], gate_weight.shape[1])
    partial_value = jnp.dot(
        hidden.reshape(-1, hidden.shape[-1]), down_weight, preferred_element_type=jnp.float32
    )
    partial_value = partial_value.reshape(expert_count, capacity, down_weight.shape[1])
    summed = lax.psum_scatter(
        partial_value.astype(jnp.bfloat16), "tp", scatter_dimension=2, tiled=True
    )
    returned = lax.all_to_all(summed, "ep", split_axis=0, concat_axis=0, tiled=True)
    picked = returned.reshape(expert_count * capacity, -1)[target].astype(jnp.float32)
    picked = picked.reshape(row_count, top_count, -1)
    shares = expert_weights / jnp.sum(expert_weights, axis=1, keepdims=True)
    return jnp.sum(picked * shares[:, :, None], axis=1).astype(jnp.bfloat16)


def on_device(
    tokens_a,
    attn_gain,
    w_query,
    w_query_rot,
    w_latent,
    w_key_rot,
    latent_gain,
    w_key_up,
    w_value_up,
    w_output,
    tokens_b,
    ffn_gain,
    expert_ids,
    expert_weights,
    w_gate,
    w_up,
    w_down,
):
    mixed_a = attention_half(
        tokens_a,
        attn_gain,
        w_query,
        w_query_rot,
        w_latent,
        w_key_rot,
        latent_gain,
        w_key_up,
        w_value_up,
        w_output,
    )
    mixed_b = expert_half(tokens_b, ffn_gain, expert_ids, expert_weights, w_gate, w_up, w_down)
    return (mixed_a, mixed_b)


def solution(mesh):
    placed = (
        P("ep", None),
        P(),
        P(None, "tp"),
        P(None, "tp"),
        P(),
        P(),
        P(),
        P(None, "tp"),
        P(None, "tp"),
        P("tp", None),
        P("ep", None),
        P(),
        P("ep", None),
        P("ep", None),
        P("ep", None, "tp"),
        P("ep", None, "tp"),
        P("ep", "tp", None),
    )
    return jax.shard_map(
        on_device,
        mesh=mesh,
        in_specs=placed,
        out_specs=(P(("ep", "tp"), None), P("ep", "tp")),
        check_vma=False,
    )
```

profile of v0, /device:TPU:8, one launch (start us, length us, event | category | flops | bytes accessed | tf_op | source)
XLA Modules:
  0.0 389.7 jit_solution(2353448182346201327)
XLA Ops:
  9.4 2.4 multiply_reduce_fusion.2
  11.8 2.0 convolution_convert_fusion.4
  13.9 2.0 convolution_convert_fusion.2
  19.6 2.4 scatter_custom_fusion.1
  22.1 2.4 scatter_custom_fusion
  27.7 6.0 %gather_fusion = bf16[1024,2048]{1,0:T(8,128)(2,1)} fusion(bf16[256,2048]{1,0:T(8,128)(2,1)S(1)} %fusion.21, s32[1024]{0:T(1024)S(1)} %fusion.47), kind=kCustom, calls=%fused_computation | custom fusion | bytes 8392704 | tf_op jit(solution)/shard_map/gather | solution.py:134
  33.7 4.6 %broadcast_select_fusion = bf16[64,16,2048]{2,1,0:T(8,128)(2,1)} fusion(bf16[64,16,2048]{2,1,0:T(8,128)(2,1)} %bitcast.79, pred[64,16]{1,0:T(8,128)(4,1)S(1)} %broadcast_in_dim.76), kind=kLoop, calls=%fused_computation.19 | loop fusion | flops 2097152 | bytes 8389632 | tf_op jit(solution)/shard_map/jit(_where)/select_n | solution.py:134
  38.3 12.3 %all-to-all-start = ((bf16[64,16,2048]{2,1,0:T(8,128)(2,1)}), bf16[64,16,2048]{2,1,0:T(8,128)(2,1)}, u32[]{:S(2)}, u32[]{:S(2)}) async-start(bf16[64,16,2048]{2,1,0:T(8,128)(2,1)} %broadcast_select_fusion), calls=%async_computation.1 | async-start | bytes 8388608 | tf_op jit(solution)/shard_map/all_to_all | solution.py:139
  51.2 154.9 %all-gather = bf16[8192,1,32]{0,2,1:T(8,128)(2,1)S(1)} all-gather(bf16[128,1,32]{0,2,1:T(8,128)(2,1)S(1)} %pad_maximum_fusion), channel_id=2, replica_groups=mesh['ep'=64,'tp'=4] {'ep'}, dimensions={0}, use_global_device_ids=true | all-gather | bytes 532480 | tf_op jit(solution)/shard_map/all_gather | solution.py:74
  208.0 2.1 convolution_convert_fusion.3
  210.1 4.2 %fusion.28 = f32[1024,256]{1,0:T(8,128)S(1)} fusion(bf16[1024,2048]{1,0:T(8,128)(2,1)} %bitcast.15, bf16[1,2048,256]{2,1,0:T(8,128)(2,1)} %param.31), kind=kOutput, calls=%fused_computation.41 | convolution fusion | flops 1073741824 | bytes 6291456 | tf_op jit(solution)/shard_map/dot_general | solution.py:141
  214.4 3.9 fusion.22
  218.3 3.2 convolution_convert_fusion
  224.2 14.9 %fusion.30 = f32[128,8,64,128]{0,3,2,1:T(8,128)} fusion(bf16[64,128,32]{1,0,2:T(8,128)(2,1)} %bitcast.80, bf16[128,8,16]{0,2,1:T(8,128)(2,1)S(1)} %get-tuple-element.7, bf16[128,8,16]{0,2,1:T(8,128)(2,1)S(1)} %get-tuple-element.6), kind=kOutput, calls=%fused_computation.44 | convolution fusion | flops 537001984 | bytes 34144256 | tf_op jit(solution)/shard_map/yjx,inx->yjin/dot_general | solution.py:79
  239.1 21.2 %reshape.303 = bf16[64,128,8,64]{3,2,1,0:T(8,128)(2,1)} reshape(bf16[8192,512]{1,0:T(8,128)(2,1)} %all-gather.4.cloned.1.call-done) | data formatting | bytes 16777216 | tf_op jit(solution)/shard_map/reshape | solution.py:72
  260.4 21.2 %reshape.304 = bf16[64,128,8,64]{3,2,1,0:T(8,128)(2,1)} reshape(bf16[8192,512]{1,0:T(8,128)(2,1)} %all-gather.6.cloned.1.call-done) | data formatting | bytes 16777216 | tf_op jit(solution)/shard_map/reshape | solution.py:73
  281.6 27.4 %fusion.64 = (f32[128,8,64]{0,2,1:T(8,128)S(1)}, f32[128,8,64,128]{0,3,2,1:T(8,128)}) fusion(f32[128,8,64,128]{0,3,2,1:T(8,128)} %fusion.30, bf16[128,8,64,1]{0,2,3,1:T(8,128)(2,1)S(1)} %bitcast.82, bf16[64,128,8,64]{3,2,1,0:T(8,128)(2,1)} %reshape.303, pred[128,64,128]{0,2,1:T(8,128)(4,1)S(1)} %broadcast_compare_fusion), kind=kOutput, calls=%fused_computation.109 | convolution fusion | flops 1107230720 | bytes 76939264 | tf_op jit(solution)/shard_map/yvz,wrvz->yvwr/dot_general | solution.py:78
  309.0 16.1 %fusion.2 = (f32[128,8,64]{0,2,1:T(8,128)S(1)}, f32[128,8]{0,1:T(8,128)S(1)}) fusion(f32[128,8,64,128]{0,3,2,1:T(8,128)} %get-tuple-element.15, f32[128,8,64]{0,2,1:T(8,128)S(1)} %get-tuple-element.14, pred[128,64,128]{0,2,1:T(8,128)(4,1)S(1)} %broadcast_compare_fusion), kind=kLoop, calls=%fused_computation.8 | loop fusion | flops 33487872 | bytes 35131392 | tf_op jit(solution)/shard_map/reduce_sum | solution.py:91
  325.9 8.3 %all-to-all-start.1 = ((bf16[64,16,512]{2,1,0:T(8,128)(2,1)}), bf16[64,16,512]{2,1,0:T(8,128)(2,1)}, u32[]{:S(2)}, u32[]{:S(2)}) async-start(bf16[64,16,512]{2,1,0:T(8,128)(2,1)} %reduce-scatter.5.cloned.1.call-done), calls=%async_computation.3 | async-start | bytes 2097152 | tf_op jit(solution)/shard_map/all_to_all | solution.py:152
  334.2 20.3 %fusion.6 = f32[128,8,64]{0,2,1:T(8,128)} fusion(f32[128,8,64]{0,2,1:T(8,128)} %get-tuple-element.5, f32[128,8,64,128]{0,3,2,1:T(8,128)} %get-tuple-element.15, f32[128,8,64]{0,2,1:T(8,128)S(1)} %get-tuple-element.14, pred[128,64,128]{0,2,1:T(8,128)(4,1)S(1)} %broadcast_compare_fusion, bf16[64,128,8,64]{3,2,1,0:T(8,128)(2,1)} %reshape.304), kind=kOutput, calls=%fused_computation.12 | convolution fusion | flops 1107230720 | bytes 43778048 | tf_op jit(solution)/shard_map/qhbk,bkhd->qhbd/dot_general | solution.py:92
  357.0 5.8 %all-to-all-done.1 = bf16[64,16,512]{2,1,0:T(8,128)(2,1)} async-done(((bf16[64,16,512]{2,1,0:T(8,128)(2,1)}), bf16[64,16,512]{2,1,0:T(8,128)(2,1)}, u32[]{:S(2)}, u32[]{:S(2)}) %all-to-all-start.1) | async-done | bytes 1048608 | tf_op jit(solution)/shard_map/all_to_all | solution.py:152
  362.9 4.0 %gather_fusion.1 = bf16[512,512]{1,0:T(8,128)(2,1)} fusion(bf16[1024,512]{1,0:T(8,128)(2,1)} %bitcast.21, s32[1024]{0:T(1024)S(1)} %pad_clamp_fusion), kind=kCustom, calls=%fused_computation.1 | custom fusion | bytes 1050624 | tf_op jit(solution)/shard_map/gather | solution.py:153
  368.6 2.1 multiply_reduce_fusion
  370.6 11.7 %reduce-scatter.3.cloned.1.call-done = bf16[32,2048]{1,0:T(8,128)(2,1)} async-done(((bf16[128,2048]{1,0:T(8,128)(2,1)}), bf16[32,2048]{1,0:T(8,128)(2,1)}) %reduce-scatter.3.cloned.1.call-update) | async-done | bytes 131088 | tf_op jit(solution)/shard_map/reduce_scatter | solution.py:106
  (70 shorter events, 18.5 us)
Async XLA Ops:
  8.0 347.5 %copy-start = (bf16[512,2048]{1,0:T(8,128)(2,1)S(1)}, bf16[512,2048]{1,0:T(8,128)(2,1)}, u32[]{:S(2)}) copy-start(bf16[512,2048]{1,0:T(8,128)(2,1)} %param.26) | copy-start | bytes 6291460
  8.0 231.1 %all-gather.4.cloned.1.call-start = ((), (), s32[]{:S(2)}) async-start(), calls=%async_computation.4 | async-start | bytes 8519680 | tf_op jit(solution)/shard_map/all_gather | solution.py:68
  13.8 246.5 %all-gather.6.cloned.1.call-start = ((), (), s32[]{:S(2)}) async-start(), calls=%async_computation.5 | async-start | bytes 8519680 | tf_op jit(solution)/shard_map/all_gather | solution.py:69
  33.7 16.9 %copy-start.2 = (bf16[128,2048]{1,0:T(8,128)(2,1)S(1)}, bf16[128,2048]{1,0:T(8,128)(2,1)}, u32[]{:S(2)}) copy-start(bf16[128,2048]{1,0:T(8,128)(2,1)} %param.17) | copy-start | bytes 1572868
  33.7 16.9 %copy-start.4 = (bf16[2048,32]{0,1:T(8,128)(2,1)S(1)}, bf16[2048,32]{0,1:T(8,128)(2,1)}, u32[]{:S(2)}) copy-start(bf16[2048,32]{0,1:T(8,128)(2,1)} %param.22) | copy-start | bytes 393220
  33.7 17.0 %copy-start.5 = (f32[2048]{0:T(1024)S(1)}, f32[2048]{0:T(1024)}, u32[]{:S(2)}) copy-start(f32[2048]{0:T(1024)} %param.18) | copy-start | bytes 24580
  38.3 171.8 %all-to-all-start = ((bf16[64,16,2048]{2,1,0:T(8,128)(2,1)}), bf16[64,16,2048]{2,1,0:T(8,128)(2,1)}, u32[]{:S(2)}, u32[]{:S(2)}) async-start(bf16[64,16,2048]{2,1,0:T(8,128)(2,1)} %broadcast_select_fusion), calls=%async_computation.1 | async-start | bytes 8388608 | tf_op jit(solution)/shard_map/all_to_all | solution.py:139
  50.6 275.3 %reduce-scatter.5.cloned.1.call-start = ((), (), s32[]{:S(2)}) async-start(), calls=%async_computation.7 | async-start | bytes 5242880 | tf_op jit(solution)/shard_map/reduce_scatter | solution.py:149
  210.1 8.1 %copy-start.1 = (bf16[1,256,2048]{2,1,0:T(8,128)(2,1)S(1)}, bf16[1,256,2048]{2,1,0:T(8,128)(2,1)}, u32[]{:S(2)}) copy-start(bf16[1,256,2048]{2,1,0:T(8,128)(2,1)} %param.33) | copy-start | bytes 3145732
  325.9 37.0 %all-to-all-start.1 = ((bf16[64,16,512]{2,1,0:T(8,128)(2,1)}), bf16[64,16,512]{2,1,0:T(8,128)(2,1)}, u32[]{:S(2)}, u32[]{:S(2)}) async-start(bf16[64,16,512]{2,1,0:T(8,128)(2,1)} %reduce-scatter.5.cloned.1.call-done), calls=%async_computation.3 | async-start | bytes 2097152 | tf_op jit(solution)/shard_map/all_to_all | solution.py:152
  334.2 48.1 %reduce-scatter.3.cloned.1.call-start = ((), (), s32[]{:S(2)}) async-start(), calls=%async_computation.6 | async-start | bytes 655360 | tf_op jit(solution)/shard_map/reduce_scatter | solution.py:106
  334.2 22.6 %copy-start.3 = (f32[256,2]{0,1:T(2,128)S(1)}, f32[256,2]{0,1:T(2,128)}, u32[]{:S(2)}) copy-start(f32[256,2]{0,1:T(2,128)} %param.30) | copy-start | bytes 6148
Sparse Core Ops, SparseCore 0:
  13.9 129.2 all-gather.3
  146.6 82.3 all-gather.5
Sparse Core Ops, SparseCore 1:
  221.6 48.2 reduce-scatter.4
  356.9 25.3 reduce-scatter.2
where the time goes:
time: 392 us; the launch traced here: 390 us
  blocking collectives  155 us (40%)
  matrix products  85.8 us (22%)
  local copies, waits for them, and re-layouts  61.9 us (16%)
  other arithmetic  33 us (8%)
  starting transfers between devices  20.7 us (5%)
  waiting for transfers between devices  17.6 us (4%)
  between operations  15.8 us (4%)
    all_gather x1, blocking collectives, attention_half(): lax.all_gather(key_turned, 'ep', axis=0, tiled=True)  155 us
    dot_general x1, matrix products, attention_half(): jnp.einsum('yvz,wrvz->yvwr', query_plain, key_blocks, preferred_element_t...  27.4 us
    reshape x1, local copies, waits for them, and re-layouts, attention_half(): key_blocks = update_key_plain.reshape(blocks, row_count, head_count, NOPE)  21.2 us
    reshape x1, local copies, waits for them, and re-layouts, attention_half(): value_blocks = update_values.reshape(blocks, row_count, head_count, VD)  21.2 us
    dot_general x1, matrix products, attention_half(): jnp.einsum('qhbk,bkhd->qhbd', probs.astype(jnp.bfloat16), value_blocks, p...  20.3 us
    reduce_sum x1, other arithmetic, attention_half(): block_total = jnp.sum(probs, axis=-1)  16.1 us
    dot_general x1, matrix products, attention_half(): jnp.einsum('yjx,inx->yjin', query_rotated_rows, rotated_key_blocks, prefe...  14.9 us
    all_to_all x1, starting transfers between devices, expert_half(): lax.all_to_all(outgoing, 'ep', split_axis=0, concat_axis=0, tiled=True)  12.3 us
  transfers between devices with their start and end apart: 6, of which 2 were waited for; matrix products, arithmetic and copies ran while one was open for 45% of the time, Pallas kernels for 0%

commit v1 on v0

--- a/solution.py
+++ b/solution.py
@@ -8,6 +8,12 @@
 VD = 64
 epsilon = 1e-06
 rope_base = 10000.0
+
+
+def gather_by_exchange(x, axis, dim):
+    count = lax.axis_size(axis)
+    repeats = [count if d == dim else 1 for d in range(x.ndim)]
+    return lax.all_to_all(jnp.tile(x, repeats), axis, split_axis=dim, concat_axis=dim, tiled=True)
 
 
 def normalize(matrix, gain):
@@ -71,9 +77,7 @@
     blocks = key_count // row_count
     key_blocks = update_key_plain.reshape(blocks, row_count, head_count, NOPE)
     value_blocks = update_values.reshape(blocks, row_count, head_count, VD)
-    rotated_key_blocks = lax.all_gather(key_turned, "ep", axis=0, tiled=True).reshape(
-        blocks, row_count, ROPE
-    )
+    rotated_key_blocks = gather_by_exchange(key_turned, "ep", 0).reshape(blocks, row_count, ROPE)
     score_matrix = (
         jnp.einsum("yvz,wrvz->yvwr", query_plain, key_blocks, preferred_element_type=jnp.float32)
         + jnp.einsum(

time: 392 us -> 361 us (0.921)
  blocking collectives: 155 us -> 0 us
  waiting for transfers between devices: 17.6 us -> 135 us
  starting transfers between devices: 20.7 us -> 27 us
    all_gather x1 -> x0, blocking collectives: 155 us -> none  [attention_half(): lax.all_gather(key_turned, 'ep', axis=0, tiled=True)]
    all_to_all x1, waiting for transfers between devices: 0.01 us -> 110 us  [expert_half(): lax.all_to_all(outgoing, 'ep', split_axis=0, concat_axis=0, tiled=True)]
    all_to_all x0 -> x1, starting transfers between devices: none -> 6.84 us  [gather_by_exchange(): lax.all_to_all(jnp.tile(x, repeats), axis, split_axis=dim, concat_axis=di...]
    all_to_all x0 -> x1, waiting for transfers between devices: none -> 6.57 us  [gather_by_exchange(): lax.all_to_all(jnp.tile(x, repeats), axis, split_axis=dim, concat_axis=di...]
  transfers between devices with their start and end apart: 6 -> 7, of which waited for: 2 -> 5; matrix products, arithmetic and copies ran while one was open for 45% -> 49% of each run, Pallas kernels for 0% -> 0%
where the time goes in v1:
time: 361 us; the launch traced here: 359 us
  waiting for transfers between devices  135 us (37%)
  matrix products  85.8 us (24%)
  local copies, waits for them, and re-layouts  62.1 us (17%)
  other arithmetic  32.8 us (9%)
  starting transfers between devices  27 us (7%)
  between operations  15.8 us (4%)
    all_to_all x1, waiting for transfers between devices, expert_half(): lax.all_to_all(outgoing, 'ep', split_axis=0, concat_axis=0, tiled=True)  110 us
    dot_general x1, matrix products, attention_half(): jnp.einsum('yvz,wrvz->yvwr', query_plain, key_blocks, preferred_element_t...  27.4 us
    reshape x1, local copies, waits for them, and re-layouts, attention_half(): key_blocks = update_key_plain.reshape(blocks, row_count, head_count, NOPE)  21.5 us
    reshape x1, local copies, waits for them, and re-layouts, attention_half(): value_blocks = update_values.reshape(blocks, row_count, head_count, VD)  21.2 us
    dot_general x1, matrix products, attention_half(): jnp.einsum('qhbk,bkhd->qhbd', probs.astype(jnp.bfloat16), value_blocks, p...  20 us
    reduce_sum x1, other arithmetic, attention_half(): block_total = jnp.sum(probs, axis=-1)  16.1 us
    dot_general x1, matrix products, attention_half(): jnp.einsum('yjx,inx->yjin', query_rotated_rows, rotated_key_blocks, prefe...  16.1 us
    all_to_all x1, starting transfers between devices, expert_half(): lax.all_to_all(outgoing, 'ep', split_axis=0, concat_axis=0, tiled=True)  12.3 us
  transfers between devices with their start and end apart: 7, of which 5 were waited for; matrix products, arithmetic and copies ran while one was open for 49% of the time, Pallas kernels for 0%

profile of v1, /device:TPU:8, one launch (start us, length us, event | category | flops | bytes accessed | tf_op | source)
XLA Modules:
  0.0 358.7 jit_solution(8720664844643153763)
XLA Ops:
  9.4 2.4 multiply_reduce_fusion.2
  19.6 2.4 scatter_custom_fusion.1
  22.1 2.4 scatter_custom_fusion
  27.7 6.0 %gather_fusion = bf16[1024,2048]{1,0:T(8,128)(2,1)} fusion(bf16[256,2048]{1,0:T(8,128)(2,1)S(1)} %fusion.21, s32[1024]{0:T(1024)S(1)} %fusion.46), kind=kCustom, calls=%fused_computation | custom fusion | bytes 8392704 | tf_op jit(solution)/shard_map/gather | solution.py:138
  33.7 4.6 %broadcast_select_fusion = bf16[64,16,2048]{2,1,0:T(8,128)(2,1)} fusion(bf16[64,16,2048]{2,1,0:T(8,128)(2,1)} %bitcast.76, pred[64,16]{1,0:T(8,128)(4,1)S(1)} %broadcast_in_dim.76), kind=kLoop, calls=%fused_computation.19 | loop fusion | flops 2097152 | bytes 8389632 | tf_op jit(solution)/shard_map/jit(_where)/select_n | solution.py:138
  38.3 12.3 %all-to-all-start.1 = ((bf16[64,16,2048]{2,1,0:T(8,128)(2,1)}), bf16[64,16,2048]{2,1,0:T(8,128)(2,1)}, u32[]{:S(2)}, u32[]{:S(2)}) async-start(bf16[64,16,2048]{2,1,0:T(8,128)(2,1)} %broadcast_select_fusion), calls=%async_computation.2 | async-start | bytes 8388608 | tf_op jit(solution)/shard_map/all_to_all | solution.py:143
  53.1 2.1 convolution_convert_fusion.3
  55.2 110.3 %all-to-all-done.1 = bf16[64,16,2048]{2,1,0:T(8,128)(2,1)} async-done(((bf16[64,16,2048]{2,1,0:T(8,128)(2,1)}), bf16[64,16,2048]{2,1,0:T(8,128)(2,1)}, u32[]{:S(2)}, u32[]{:S(2)}) %all-to-all-start.1) | async-done | bytes 4194336 | tf_op jit(solution)/shard_map/all_to_all | solution.py:143
  166.4 6.8 %all-to-all-start = ((bf16[64,128,32]{1,2,0:T(8,128)(2,1)}), bf16[64,128,32]{1,2,0:T(8,128)(2,1)}, u32[]{:S(2)}, u32[]{:S(2)}) async-start(bf16[64,128,32]{1,2,0:T(8,128)(2,1)} %tile.2), calls=%async_computation | async-start | bytes 1048576 | tf_op jit(solution)/shard_map/all_to_all | solution.py:16
  173.5 3.8 %fusion.28 = f32[1024,256]{1,0:T(8,128)S(1)} fusion(bf16[1024,2048]{1,0:T(8,128)(2,1)} %bitcast.16, bf16[1,2048,256]{2,1,0:T(8,128)(2,1)} %param.31), kind=kOutput, calls=%fused_computation.41 | convolution fusion | flops 1073741824 | bytes 6291456 | tf_op jit(solution)/shard_map/dot_general | solution.py:145
  177.3 3.5 fusion.22
  180.8 3.2 convolution_convert_fusion
  185.6 6.6 %all-to-all-done = bf16[64,128,32]{1,2,0:T(8,128)(2,1)} async-done(((bf16[64,128,32]{1,2,0:T(8,128)(2,1)}), bf16[64,128,32]{1,2,0:T(8,128)(2,1)}, u32[]{:S(2)}, u32[]{:S(2)}) %all-to-all-start) | async-done | bytes 524320 | tf_op jit(solution)/shard_map/all_to_all | solution.py:16
  192.2 16.1 %fusion.30 = f32[128,8,64,128]{0,3,2,1:T(8,128)} fusion(bf16[64,128,32]{1,2,0:T(8,128)(2,1)} %all-to-all-done, bf16[128,8,16]{0,2,1:T(8,128)(2,1)S(1)} %get-tuple-element.7, bf16[128,8,16]{0,2,1:T(8,128)(2,1)S(1)} %get-tuple-element.6), kind=kOutput, calls=%fused_computation.44 | convolution fusion | flops 537001984 | bytes 34144256 | tf_op jit(solution)/shard_map/yjx,inx->yjin/dot_general | solution.py:83
  208.2 21.5 %reshape.310 = bf16[64,128,8,64]{3,2,1,0:T(8,128)(2,1)} reshape(bf16[8192,512]{1,0:T(8,128)(2,1)} %all-gather.3.cloned.1.call-done) | data formatting | bytes 16777216 | tf_op jit(solution)/shard_map/reshape | solution.py:78
  230.6 21.2 %reshape.311 = bf16[64,128,8,64]{3,2,1,0:T(8,128)(2,1)} reshape(bf16[8192,512]{1,0:T(8,128)(2,1)} %all-gather.5.cloned.1.call-done) | data formatting | bytes 16777216 | tf_op jit(solution)/shard_map/reshape | solution.py:79
  251.8 27.4 %fusion.63 = (f32[128,8,64]{0,2,1:T(8,128)S(1)}, f32[128,8,64,128]{0,3,2,1:T(8,128)}) fusion(f32[128,8,64,128]{0,3,2,1:T(8,128)} %fusion.30, bf16[128,8,64,1]{0,2,3,1:T(8,128)(2,1)S(1)} %bitcast.77, bf16[64,128,8,64]{3,2,1,0:T(8,128)(2,1)} %reshape.310, pred[128,64,128]{0,2,1:T(8,128)(4,1)S(1)} %broadcast_compare_fusion), kind=kOutput, calls=%fused_computation.108 | convolution fusion | flops 1107230720 | bytes 76939264 | tf_op jit(solution)/shard_map/yvz,wrvz->yvwr/dot_general | solution.py:82
  279.3 16.1 %fusion.2 = (f32[128,8,64]{0,2,1:T(8,128)S(1)}, f32[128,8]{0,1:T(8,128)S(1)}) fusion(f32[128,8,64,128]{0,3,2,1:T(8,128)} %get-tuple-element.15, f32[128,8,64]{0,2,1:T(8,128)S(1)} %get-tuple-element.14, pred[128,64,128]{0,2,1:T(8,128)(4,1)S(1)} %broadcast_compare_fusion), kind=kLoop, calls=%fused_computation.8 | loop fusion | flops 33487872 | bytes 35131392 | tf_op jit(solution)/shard_map/reduce_sum | solution.py:95
  296.2 7.5 %all-to-all-start.2 = ((bf16[64,16,512]{2,1,0:T(8,128)(2,1)}), bf16[64,16,512]{2,1,0:T(8,128)(2,1)}, u32[]{:S(2)}, u32[]{:S(2)}) async-start(bf16[64,16,512]{2,1,0:T(8,128)(2,1)} %reduce-scatter.5.cloned.1.call-done), calls=%async_computation.4 | async-start | bytes 2097152 | tf_op jit(solution)/shard_map/all_to_all | solution.py:156
  303.7 20.0 %fusion.6 = f32[128,8,64]{0,2,1:T(8,128)} fusion(f32[128,8,64]{0,2,1:T(8,128)} %get-tuple-element.5, f32[128,8,64,128]{0,3,2,1:T(8,128)} %get-tuple-element.15, f32[128,8,64]{0,2,1:T(8,128)S(1)} %get-tuple-element.14, pred[128,64,128]{0,2,1:T(8,128)(4,1)S(1)} %broadcast_compare_fusion, bf16[64,128,8,64]{3,2,1,0:T(8,128)(2,1)} %reshape.311), kind=kOutput, calls=%fused_computation.12 | convolution fusion | flops 1107230720 | bytes 43778048 | tf_op jit(solution)/shard_map/qhbk,bkhd->qhbd/dot_general | solution.py:96
  326.2 6.1 %all-to-all-done.2 = bf16[64,16,512]{2,1,0:T(8,128)(2,1)} async-done(((bf16[64,16,512]{2,1,0:T(8,128)(2,1)}), bf16[64,16,512]{2,1,0:T(8,128)(2,1)}, u32[]{:S(2)}, u32[]{:S(2)}) %all-to-all-start.2) | async-done | bytes 1048608 | tf_op jit(solution)/shard_map/all_to_all | solution.py:156
  332.3 4.0 %gather_fusion.1 = bf16[512,512]{1,0:T(8,128)(2,1)} fusion(bf16[1024,512]{1,0:T(8,128)(2,1)} %bitcast.22, s32[1024]{0:T(1024)S(1)} %pad_clamp_fusion), kind=kCustom, calls=%fused_computation.1 | custom fusion | bytes 1050624 | tf_op jit(solution)/shard_map/gather | solution.py:157
  338.0 2.1 multiply_reduce_fusion
  340.1 11.2 %reduce-scatter.3.cloned.1.call-done = bf16[32,2048]{1,0:T(8,128)(2,1)} async-done(((bf16[128,2048]{1,0:T(8,128)(2,1)}), bf16[32,2048]{1,0:T(8,128)(2,1)}) %reduce-scatter.3.cloned.1.call-update) | async-done | bytes 131088 | tf_op jit(solution)/shard_map/reduce_scatter | solution.py:110
  (73 shorter events, 23.3 us)
Async XLA Ops:
  8.0 316.8 %copy-start = (bf16[512,2048]{1,0:T(8,128)(2,1)S(1)}, bf16[512,2048]{1,0:T(8,128)(2,1)}, u32[]{:S(2)}) copy-start(bf16[512,2048]{1,0:T(8,128)(2,1)} %param.26) | copy-start | bytes 6291460
  8.0 200.2 %all-gather.3.cloned.1.call-start = ((), (), s32[]{:S(2)}) async-start(), calls=%async_computation.5 | async-start | bytes 8519680 | tf_op jit(solution)/shard_map/all_gather | solution.py:74
  13.8 216.8 %all-gather.5.cloned.1.call-start = ((), (), s32[]{:S(2)}) async-start(), calls=%async_computation.6 | async-start | bytes 8519680 | tf_op jit(solution)/shard_map/all_gather | solution.py:75
  33.7 16.9 %copy-start.2 = (bf16[128,2048]{1,0:T(8,128)(2,1)S(1)}, bf16[128,2048]{1,0:T(8,128)(2,1)}, u32[]{:S(2)}) copy-start(bf16[128,2048]{1,0:T(8,128)(2,1)} %param.17) | copy-start | bytes 1572868
  33.7 16.9 %copy-start.5 = (bf16[2048,32]{0,1:T(8,128)(2,1)S(1)}, bf16[2048,32]{0,1:T(8,128)(2,1)}, u32[]{:S(2)}) copy-start(bf16[2048,32]{0,1:T(8,128)(2,1)} %param.22) | copy-start | bytes 393220
  33.7 16.9 %copy-start.6 = (f32[2048]{0:T(1024)S(1)}, f32[2048]{0:T(1024)}, u32[]{:S(2)}) copy-start(f32[2048]{0:T(1024)} %param.18) | copy-start | bytes 24580
  38.3 127.2 %all-to-all-start.1 = ((bf16[64,16,2048]{2,1,0:T(8,128)(2,1)}), bf16[64,16,2048]{2,1,0:T(8,128)(2,1)}, u32[]{:S(2)}, u32[]{:S(2)}) async-start(bf16[64,16,2048]{2,1,0:T(8,128)(2,1)} %broadcast_select_fusion), calls=%async_computation.2 | async-start | bytes 8388608 | tf_op jit(solution)/shard_map/all_to_all | solution.py:143
  166.4 10.9 %copy-start.4 = (bf16[1,2048,256]{2,1,0:T(8,128)(2,1)S(1)}, bf16[1,2048,256]{2,1,0:T(8,128)(2,1)}, u32[]{:S(2)}) copy-start(bf16[1,2048,256]{2,1,0:T(8,128)(2,1)} %param.32) | copy-start | bytes 3145732
  166.4 25.8 %all-to-all-start = ((bf16[64,128,32]{1,2,0:T(8,128)(2,1)}), bf16[64,128,32]{1,2,0:T(8,128)(2,1)}, u32[]{:S(2)}, u32[]{:S(2)}) async-start(bf16[64,128,32]{1,2,0:T(8,128)(2,1)} %tile.2), calls=%async_computation | async-start | bytes 1048576 | tf_op jit(solution)/shard_map/all_to_all | solution.py:16
  173.2 122.9 %reduce-scatter.5.cloned.1.call-start = ((), (), s32[]{:S(2)}) async-start(), calls=%async_computation.8 | async-start | bytes 5242880 | tf_op jit(solution)/shard_map/reduce_scatter | solution.py:153
  173.5 7.3 %copy-start.1 = (bf16[1,256,2048]{2,1,0:T(8,128)(2,1)S(1)}, bf16[1,256,2048]{2,1,0:T(8,128)(2,1)}, u32[]{:S(2)}) copy-start(bf16[1,256,2048]{2,1,0:T(8,128)(2,1)} %param.33) | copy-start | bytes 3145732
  296.2 36.2 %all-to-all-start.2 = ((bf16[64,16,512]{2,1,0:T(8,128)(2,1)}), bf16[64,16,512]{2,1,0:T(8,128)(2,1)}, u32[]{:S(2)}, u32[]{:S(2)}) async-start(bf16[64,16,512]{2,1,0:T(8,128)(2,1)} %reduce-scatter.5.cloned.1.call-done), calls=%async_computation.4 | async-start | bytes 2097152 | tf_op jit(solution)/shard_map/all_to_all | solution.py:156
  303.7 47.6 %reduce-scatter.3.cloned.1.call-start = ((), (), s32[]{:S(2)}) async-start(), calls=%async_computation.7 | async-start | bytes 655360 | tf_op jit(solution)/shard_map/reduce_scatter | solution.py:110
  303.7 22.3 %copy-start.3 = (f32[256,2]{0,1:T(2,128)S(1)}, f32[256,2]{0,1:T(2,128)}, u32[]{:S(2)}) copy-start(f32[256,2]{0,1:T(2,128)} %param.30) | copy-start | bytes 6148
Sparse Core Ops, SparseCore 0:
  13.9 129.3 all-gather.2
  146.6 83.9 all-gather.4
Sparse Core Ops, SparseCore 1:
  184.1 50.4 reduce-scatter.4
  326.1 25.1 reduce-scatter.2
